TPU v7x, 512 devices: a whole 4x4x16 slice. The times are simulated.
512 devices in a mesh: rep: 2 (over z_hi), fs: 32 (over z_lo, y), tp: 8 (over x, core).
Axes of the slice: x: 4, y: 4, z: 16 (z_hi: 2, z_lo: 8; z = z_hi * 8 + z_lo), core: 2. Of those that a mesh axis runs over, the one named last changes fastest.
Arguments:
- tokens_in: bfloat16 [16384, 2048], P(('rep', 'fs', 'tp')), may hold values from -6 to 6
- norm_gains: float32 [3, 2048], replicated, may hold values from 0.1 to 1.9
- gate_w: float32 [2048, 3072], P('fs', 'tp'), may hold values from -0.125 to 0.125
- gate_scale: float32 [3072], P('tp'), may hold values from 0.5 to 2
- up_w: float32 [2048, 3072], P('fs', 'tp'), may hold values from -0.125 to 0.125
- up_scale: float32 [3072], P('tp'), may hold values from 0.5 to 2
- down_w: float32 [3072, 2048], P('tp', 'fs'), may hold values from -0.109375 to 0.109375
- down_scale: float32 [2048], P('fs'), may hold values from 0.5 to 2
- query_w: float32 [2048, 2048], P('fs', 'tp'), may hold values from -0.125 to 0.125
- query_scale: float32 [2048], P('tp'), may hold values from 0.5 to 2
- key_w: float32 [2048, 2048], P('fs', 'tp'), may hold values from -0.125 to 0.125
- key_scale: float32 [2048], P('tp'), may hold values from 0.5 to 2
- value_w: float32 [2048, 2048], P('fs', 'tp'), may hold values from -0.125 to 0.125
- value_scale: float32 [2048], P('tp'), may hold values from 0.5 to 2
- out_w: float32 [2048, 2048], P('tp', 'fs'), may hold values from -0.125 to 0.125
- out_scale: float32 [2048], P('fs'), may hold values from 0.5 to 2
- head_gain: float32 [256], replicated, may hold values from 0.1 to 1.9
- decay_rate: float32 [8], P('tp'), may hold values from 0 to 1, as said below
Outputs:
- tokens_out: bfloat16 [16384, 2048], P(('rep', 'fs', 'tp'))
Inputs may be any that keep to these rules, and one draw needn't show every extreme that they name: `decay_rate`: each head's decay per position, positive.
All inputs are finite; a program needn't handle non-finite values.
Results may differ from a plain program's by a relative error of at most 0.02.
Values may be sent and summed in bfloat16 or wider, within the bound.
No kernel may reach another device: no remote copies, remote signals or barrier semaphores. Data moves between devices by JAX's collectives and lax.ppermute only.
A program may use at most 64 MiB of HBM per device.

v0:
```python
import math
import jax
import jax.numpy as jnp
from jax import lax
from jax.sharding import PartitionSpec as P

DK = 256
DV = 256
BLOCK = 64
EPSILON = 1e-05


def gather_turned(arrays, axis, dims):
    turned = [jnp.moveaxis(a, dim, 0) for a, dim in zip(arrays, dims)]
    widths = [t[0].size for t in turned]
    both = jnp.concatenate([t.reshape(-1, w) for t, w in zip(turned, widths)], axis=1)
    result = lax.all_gather(both, axis, axis=0, tiled=True)
    blocks = jnp.split(result, [sum(widths[:k]) for k in range(1, len(widths))], axis=1)
    return tuple(
        (
            jnp.moveaxis(b.reshape(-1, *t.shape[1:]), 0, dim)
            for b, t, dim in zip(blocks, turned, dims)
        )
    )


def sent_to_all(array, axis):
    copies = jnp.broadcast_to(array, (lax.axis_size(axis), *array.shape))
    return lax.all_to_all(copies, axis, split_axis=0, concat_axis=0, tiled=True)


def in_order(blocks, dim):
    shape = list(blocks.shape[1:])
    shape[dim] *= blocks.shape[0]
    return jnp.moveaxis(blocks, 0, dim).reshape(shape)


def collect(array, axis, dim):
    blocks = sent_to_all(array, axis)
    return in_order(blocks, dim)


def in_blocks(array, dim, devices):
    shape = array.shape
    blocks = array.reshape(*shape[:dim], devices, shape[dim] // devices, *shape[dim + 1 :])
    return jnp.moveaxis(blocks, dim, 0)


def summed_on_arrival(array, axis, dim):
    blocks = in_blocks(array, dim, lax.axis_size(axis))
    arrived = lax.all_to_all(blocks, axis, split_axis=0, concat_axis=0, tiled=True)
    return arrived.astype(jnp.float32).sum(axis=0)


def in_one_piece(arrays, axis, dim, along):
    both = jnp.concatenate(arrays, axis=along)
    result, at, finished = (lax.all_gather(both, axis, axis=dim, tiled=True), 0, [])
    for a in arrays:
        finished.append(lax.slice_in_dim(result, at, at + a.shape[along], axis=along))
        at += a.shape[along]
    return tuple(finished)


def rms_scale(stream, gain):
    return stream * lax.rsqrt(jnp.mean(stream * stream, axis=-1, keepdims=True) + EPSILON) * gain


def retain(query, key_rows, value, decay_rate, head_gain):
    seq_len = query.shape[0]
    blocks = seq_len // BLOCK
    local_heads = decay_rate.shape[0]
    q_heads = query.reshape(blocks, BLOCK, local_heads, DK).transpose(0, 2, 1, 3)
    k_heads = key_rows.reshape(blocks, BLOCK, local_heads, DK).transpose(0, 2, 1, 3)
    v_heads = value.reshape(blocks, BLOCK, local_heads, DV).transpose(0, 2, 1, 3)
    offsets = jnp.arange(BLOCK, dtype=jnp.float32)
    inner_decay = jnp.exp(-decay_rate[:, None, None] * jnp.abs(offsets[:, None] - offsets[None, :]))
    query_decay = jnp.exp(-decay_rate[:, None] * offsets[None, :])[..., None]
    key_decay = jnp.exp(-decay_rate[:, None] * (BLOCK - offsets)[None, :])[..., None]
    block_decay = jnp.exp(-decay_rate * BLOCK)[:, None, None]

    def advance(state, inputs):
        q_blk, k_blk, v_blk = inputs
        scores = (
            jnp.einsum("hid,hjd->hij", q_blk, k_blk, preferred_element_type=jnp.float32)
            * inner_decay
        )
        scores = scores.astype(jnp.bfloat16)
        within = jnp.einsum("hij,hje->hie", scores, v_blk, preferred_element_type=jnp.float32)
        carried = jnp.einsum(
            "hid,hde->hie",
            q_blk.astype(jnp.float32) * query_decay,
            state,
            precision=lax.Precision.HIGHEST,
        )
        k_weighted = k_blk.astype(jnp.float32) * key_decay
        state = state * block_decay + jnp.einsum(
            "hjd,hje->hde", k_weighted, v_blk.astype(jnp.float32), precision=lax.Precision.HIGHEST
        )
        return (state, within + carried)

    initial = jnp.zeros((local_heads, DK, DV), jnp.float32)
    _, retained = lax.scan(advance, initial, (q_heads, k_heads, v_heads))
    retained = retained.transpose(0, 2, 1, 3).reshape(seq_len, local_heads, DV)
    centred = retained - jnp.mean(retained, axis=-1, keepdims=True)
    normed = (
        centred
        * lax.rsqrt(jnp.mean(centred * centred, axis=-1, keepdims=True) + EPSILON)
        * head_gain
    )
    return normed.reshape(seq_len, local_heads * DV).astype(jnp.bfloat16)


def on_device(
    tokens_in,
    norm_gains,
    gate_w,
    gate_scale,
    up_w,
    up_scale,
    down_w,
    down_scale,
    query_w,
    query_scale,
    key_w,
    key_scale,
    value_w,
    value_scale,
    out_w,
    out_scale,
    head_gain,
    decay_rate,
):
    down_cols, out_cols = gather_turned((down_scale, out_scale), "fs", (0, 0))
    gate_b = gate_w.astype(jnp.bfloat16)
    up_b = up_w.astype(jnp.bfloat16)
    down_b = down_w.astype(jnp.bfloat16)
    query_b = query_w.astype(jnp.bfloat16)
    key_b = key_w.astype(jnp.bfloat16)
    value_b = value_w.astype(jnp.bfloat16)
    out_b = out_w.astype(jnp.bfloat16)

    def gather_rows(normed):
        return collect(normed, "tp", 0)

    def return_rows(hidden, weight, scale):
        return summed_on_arrival(
            (jnp.dot(hidden, weight, preferred_element_type=jnp.float32) * scale).astype(
                jnp.bfloat16
            ),
            "tp",
            0,
        )

    def feed_forward(stream, gain, weights):
        gate_full, up_full, down_full = weights
        gathered = gather_rows(rms_scale(stream, gain).astype(jnp.bfloat16))
        gate_value = jnp.dot(gathered, gate_full, preferred_element_type=jnp.float32) * gate_scale
        up_value = jnp.dot(gathered, up_full, preferred_element_type=jnp.float32) * up_scale
        hidden = (jax.nn.silu(gate_value) * up_value).astype(jnp.bfloat16)
        return return_rows(hidden, down_full, down_cols)

    stream = tokens_in.astype(jnp.float32)
    held = gather_turned((gate_b, up_b, down_b), "fs", (0, 0, 1))
    stream = stream + 0.5 * feed_forward(stream, norm_gains[0], held)
    gathered = gather_rows(rms_scale(stream, norm_gains[1]).astype(jnp.bfloat16))
    segments = in_one_piece((query_b, key_b, value_b), "fs", 0, 1)
    query_raw, key_raw, value_raw = tuple(
        (jnp.dot(gathered, segment_w, preferred_element_type=jnp.float32) for segment_w in segments)
    )
    out_full = collect(out_b, "fs", 1)
    query = (query_raw * query_scale).astype(jnp.bfloat16)
    key_rows = (key_raw * key_scale / math.sqrt(DK)).astype(jnp.bfloat16)
    value = (value_raw * value_scale).astype(jnp.bfloat16)
    mixed = retain(query, key_rows, value, decay_rate, head_gain)
    stream = stream + return_rows(mixed, out_full, out_cols)
    stream = stream + 0.5 * feed_forward(stream, norm_gains[2], held)
    return stream.astype(jnp.bfloat16)


def solution(mesh):
    placed = (
        P(("rep", "fs", "tp"), None),
        P(),
        P("fs", "tp"),
        P("tp"),
        P("fs", "tp"),
        P("tp"),
        P("tp", "fs"),
        P("fs"),
        P("fs", "tp"),
        P("tp"),
        P("fs", "tp"),
        P("tp"),
        P("fs", "tp"),
        P("tp"),
        P("tp", "fs"),
        P("fs"),
        P(),
        P("tp"),
    )
    return jax.shard_map(
        on_device,
        mesh=mesh,
        in_specs=placed,
        out_specs=P(("rep", "fs", "tp"), None),
        check_vma=False,
    )
```

profile of v0, /device:TPU:1, one launch (start us, length us, event | category | flops | bytes accessed | tf_op | source)
XLA Modules:
  0.0 551.2 jit_solution(16911982376912300465)
XLA Ops:
  6.5 0.9 convert_bitcast_fusion
  7.4 0.9 convert_element_type.138
  8.3 0.9 convert_element_type.139
  9.2 0.7 pad_maximum_fusion
  10.0 0.8 convert_element_type.145
  10.8 0.9 convert_element_type.146
  11.7 0.8 convert_element_type.147
  12.6 0.6 pad_maximum_fusion.1
  13.2 1.0 fusion.108
  14.3 0.9 fusion.124
  15.2 1.0 fusion.110
  16.2 1.2 broadcast_in_dim.17
  17.4 10.3 %all-to-all-start = ((bf16[8,32,2048]{2,1,0:T(8,128)(2,1)}), bf16[8,32,2048]{2,1,0:T(8,128)(2,1)S(1)}, u32[]{:S(2)}, u32[]{:S(2)}) async-start(bf16[8,32,2048]{2,1,0:T(8,128)(2,1)} %broadcast_in_dim.17), calls=%async_computation | async-start | bytes 2097152 | tf_op jit(solution)/shard_map/all_to_all | solution.py:29
  27.7 107.8 %all-gather = f32[32,64,2]{1,2,0:T(2,128)S(1)} all-gather(f32[1,64,2]{1,2,0:T(2,128)S(1)} %maximum_bitcast_fusion), channel_id=1, replica_groups=mesh['rep'=2,'fs'=32,'tp'=8] {'fs'}, dimensions={0}, use_global_device_ids=true | all-gather | bytes 16896 | tf_op jit(solution)/shard_map/all_gather | solution.py:17
  135.6 87.3 %all-gather.4.cloned.1.call-done = bf16[2048,1152]{1,0:T(8,128)(2,1)} async-done(((bf16[64,1152]{1,0:T(8,128)(2,1)}), bf16[2048,1152]{1,0:T(8,128)(2,1)}) %all-gather.4.cloned.1.call-update) | async-done | bytes 4718608 | tf_op jit(solution)/shard_map/all_gather | solution.py:17
  222.9 2.1 fusion.63
  225.0 3.2 fusion.51
  228.3 40.3 %all_to_all.35 = bf16[8,32,2048]{2,1,0:T(8,128)(2,1)S(1)} all-to-all(bf16[8,32,2048]{2,1,0:T(8,128)(2,1)S(1)} %bitcast.136), channel_id=1, replica_groups=mesh['rep'=2,'fs'=32,'tp'=8] {'tp'}, dimensions={0} | all-to-all | bytes 2097152 | tf_op jit(solution)/shard_map/all_to_all | solution.py:51
  269.1 1.2 broadcast_in_dim.21
  270.3 4.5 all-to-all-start.2
  275.5 14.4 %all-to-all-done.2 = bf16[8,32,2048]{2,1,0:T(8,128)(2,1)S(1)} async-done(((bf16[8,32,2048]{2,1,0:T(8,128)(2,1)}), bf16[8,32,2048]{2,1,0:T(8,128)(2,1)S(1)}, u32[]{:S(2)}, u32[]{:S(2)}) %all-to-all-start.2) | async-done | bytes 1048608 | tf_op jit(solution)/shard_map/all_to_all | solution.py:29
  289.9 1.2 broadcast_in_dim.22
  291.1 11.8 %all-to-all-start.3 = ((bf16[32,256,64]{1,2,0:T(8,128)(2,1)}), bf16[32,256,64]{1,2,0:T(8,128)(2,1)S(1)}, u32[]{:S(2)}, u32[]{:S(2)}) async-start(bf16[32,256,64]{1,2,0:T(8,128)(2,1)} %broadcast_in_dim.22), calls=%async_computation.3 | async-start | bytes 2097152 | tf_op jit(solution)/shard_map/all_to_all | solution.py:29
  302.9 145.8 %all-gather.6.cloned.1.call-done = bf16[2048,768]{1,0:T(8,128)(2,1)} async-done(((bf16[64,768]{1,0:T(8,128)(2,1)}), bf16[2048,768]{1,0:T(8,128)(2,1)}) %all-gather.6.cloned.1.call-update) | async-done | bytes 3145744 | tf_op jit(solution)/shard_map/all_gather | solution.py:57
  448.7 1.7 fusion.92
  450.4 1.7 fusion.93
  452.1 1.7 fusion.94
  453.8 4.5 while.15
  453.8 0.3 fusion.152
  454.2 0.3 fusion.153
  454.4 0.5 fusion.151
  455.0 0.3 fusion.152
  455.3 0.3 fusion.153
  455.5 0.5 fusion.151
  456.1 0.3 fusion.152
  456.4 0.3 fusion.153
  456.7 0.5 fusion.151
  457.2 0.3 fusion.152
  457.5 0.3 fusion.153
  457.8 0.5 fusion.151
  458.5 0.2 multiply_reduce_fusion.1
  458.8 0.5 fusion.50
  459.3 41.5 %all_to_all.36 = bf16[8,32,2048]{2,1,0:T(8,128)(2,1)S(1)} all-to-all(bf16[8,32,2048]{2,1,0:T(8,128)(2,1)S(1)} %bitcast.126), channel_id=1, replica_groups=mesh['rep'=2,'fs'=32,'tp'=8] {'tp'}, dimensions={0} | all-to-all | bytes 2097152 | tf_op jit(solution)/shard_map/all_to_all | solution.py:51
  501.3 18.4 %all_to_all.37 = bf16[8,32,2048]{2,1,0:T(8,128)(2,1)S(1)} all-to-all(bf16[8,32,2048]{2,1,0:T(8,128)(2,1)S(1)} %broadcast_in_dim.23), channel_id=1, replica_groups=mesh['rep'=2,'fs'=32,'tp'=8] {'tp'}, dimensions={0} | all-to-all | bytes 2097152 | tf_op jit(solution)/shard_map/all_to_all | solution.py:29
  519.7 2.1 fusion.66
  521.8 3.3 fusion.52
  525.1 18.4 %all_to_all.38 = bf16[8,32,2048]{2,1,0:T(8,128)(2,1)S(1)} all-to-all(bf16[8,32,2048]{2,1,0:T(8,128)(2,1)S(1)} %bitcast.135), channel_id=1, replica_groups=mesh['rep'=2,'fs'=32,'tp'=8] {'tp'}, dimensions={0} | all-to-all | bytes 2097152 | tf_op jit(solution)/shard_map/all_to_all | solution.py:51
  543.7 0.7 add_convert_fusion
  (53 shorter events, 1.7 us)
Async XLA Ops:
  6.5 216.4 %all-gather.4.cloned.1.call-start = ((), (), s32[]{:S(2)}) async-start(), calls=%async_computation.7 | async-start | bytes 4866048 | tf_op jit(solution)/shard_map/all_gather | solution.py:17
  9.9 438.8 %all-gather.6.cloned.1.call-start = ((), (), s32[]{:S(2)}) async-start(), calls=%async_computation.8 | async-start | bytes 3244032 | tf_op jit(solution)/shard_map/all_gather | solution.py:57
  10.8 16.9 %copy-start.3 = (f32[64]{0:T(128)S(1)}, f32[64]{0:T(128)}, u32[]{:S(2)}) copy-start(f32[64]{0:T(128)} %param.35) | copy-start | bytes 772
  10.8 16.9 %copy-start.4 = (f32[64]{0:T(128)S(1)}, f32[64]{0:T(128)}, u32[]{:S(2)}) copy-start(f32[64]{0:T(128)} %param.27) | copy-start | bytes 772
  12.6 210.4 %copy-start.5 = (f32[384]{0:T(512)S(1)}, f32[384]{0:T(512)}, u32[]{:S(2)}) copy-start(f32[384]{0:T(512)} %param.23) | copy-start | bytes 4612
  17.4 118.2 %all-to-all-start = ((bf16[8,32,2048]{2,1,0:T(8,128)(2,1)}), bf16[8,32,2048]{2,1,0:T(8,128)(2,1)S(1)}, u32[]{:S(2)}, u32[]{:S(2)}) async-start(bf16[8,32,2048]{2,1,0:T(8,128)(2,1)} %broadcast_in_dim.17), calls=%async_computation | async-start | bytes 2097152 | tf_op jit(solution)/shard_map/all_to_all | solution.py:29
  27.7 197.4 %copy-start.6 = (f32[384]{0:T(512)S(1)}, f32[384]{0:T(512)}, u32[]{:S(2)}) copy-start(f32[384]{0:T(512)} %param.25) | copy-start | bytes 4612
  228.3 40.5 %copy-start = (bf16[32,2048]{1,0:T(8,128)(2,1)S(1)}, bf16[32,2048]{1,0:T(8,128)(2,1)}, u32[]{:S(2)}) copy-start(bf16[32,2048]{1,0:T(8,128)(2,1)} %param.20) | copy-start | bytes 393220
  268.8 6.7 %copy-start.1 = (f32[256,64]{0,1:T(8,128)S(1)}, f32[256,64]{0,1:T(8,128)}, u32[]{:S(2)}) copy-start(f32[256,64]{0,1:T(8,128)} %param.34) | copy-start | bytes 196612
  270.3 19.6 %all-to-all-start.2 = ((bf16[8,32,2048]{2,1,0:T(8,128)(2,1)}), bf16[8,32,2048]{2,1,0:T(8,128)(2,1)S(1)}, u32[]{:S(2)}, u32[]{:S(2)}) async-start(bf16[8,32,2048]{2,1,0:T(8,128)(2,1)} %broadcast_in_dim.21), calls=%async_computation.2 | async-start | bytes 2097152 | tf_op jit(solution)/shard_map/all_to_all | solution.py:29
  274.8 173.9 %copy-start.7 = (f32[256]{0:T(256)S(1)}, f32[256]{0:T(256)}, u32[]{:S(2)}) copy-start(f32[256]{0:T(256)} %param.31) | copy-start | bytes 3076
  291.1 159.4 %copy-start.8 = (f32[256]{0:T(256)S(1)}, f32[256]{0:T(256)}, u32[]{:S(2)}) copy-start(f32[256]{0:T(256)} %param.33) | copy-start | bytes 3076
  291.1 167.7 %all-to-all-start.3 = ((bf16[32,256,64]{1,2,0:T(8,128)(2,1)}), bf16[32,256,64]{1,2,0:T(8,128)(2,1)S(1)}, u32[]{:S(2)}, u32[]{:S(2)}) async-start(bf16[32,256,64]{1,2,0:T(8,128)(2,1)} %broadcast_in_dim.22), calls=%async_computation.3 | async-start | bytes 2097152 | tf_op jit(solution)/shard_map/all_to_all | solution.py:29
  448.7 3.4 copy-start.9
  453.8 5.0 copy-start.2
Sparse Core Ops, SparseCore 0:
  10.1 212.8 all-gather.3
  225.0 223.6 all-gather.5
where the time goes:
time: 552 us; the launch traced here: 551 us
  waiting for transfers between devices  248 us (45%)
  blocking collectives  226 us (41%)
  starting transfers between devices  26.7 us (5%)
  matrix products  20.6 us (4%)
  between operations  14.4 us (3%)
  other arithmetic  10.7 us (2%)
    all_gather x1, waiting for transfers between devices, in_one_piece(): lax.all_gather(both, axis, axis=dim, tiled=True)  146 us
    all_gather x1, blocking collectives, gather_turned(): result = lax.all_gather(both, axis, axis=0, tiled=True)  108 us
    all_to_all x3, blocking collectives, summed_on_arrival(): lax.all_to_all(blocks, axis, split_axis=0, concat_axis=0, tiled=True)  100 us
    all_gather x1, waiting for transfers between devices, gather_turned(): result = lax.all_gather(both, axis, axis=0, tiled=True)  87.3 us
    all_to_all x3, starting transfers between devices, sent_to_all(): return lax.all_to_all(copies, axis, split_axis=0, concat_axis=0, tiled=True)  26.6 us
    all_to_all x1, blocking collectives, sent_to_all(): return lax.all_to_all(copies, axis, split_axis=0, concat_axis=0, tiled=True)  18.4 us
    all_to_all x3, waiting for transfers between devices, sent_to_all(): return lax.all_to_all(copies, axis, split_axis=0, concat_axis=0, tiled=True)  14.4 us
  transfers between devices with their start and end apart: 5, of which 3 were waited for; matrix products, arithmetic and copies ran while one was open for 5% of the time, Pallas kernels for 0%

commit v1 on v0

--- a/solution.py
+++ b/solution.py
@@ -14,7 +14,9 @@
     turned = [jnp.moveaxis(a, dim, 0) for a, dim in zip(arrays, dims)]
     widths = [t[0].size for t in turned]
     both = jnp.concatenate([t.reshape(-1, w) for t, w in zip(turned, widths)], axis=1)
-    result = lax.all_gather(both, axis, axis=0, tiled=True)
+    result = jnp.concatenate(
+        lax.all_to_all(jnp.stack([both] * lax.axis_size(axis)), axis, 0, 0), axis=0
+    )
     blocks = jnp.split(result, [sum(widths[:k]) for k in range(1, len(widths))], axis=1)
     return tuple(
         (

time: 552 us -> 483 us (0.88)
  blocking collectives: 226 us -> 79.1 us
  waiting for transfers between devices: 248 us -> 311 us
  starting transfers between devices: 26.7 us -> 42.1 us
    all_to_all x0 -> x2, waiting for transfers between devices: none -> 242 us  [gather_turned(): lax.all_to_all(jnp.stack([both] * lax.axis_size(axis)), axis, 0, 0)]
    all_gather x1, waiting for transfers between devices: 146 us -> 0.02 us  [in_one_piece(): lax.all_gather(both, axis, axis=dim, tiled=True)]
    all_gather x1 -> x0, blocking collectives: 108 us -> none  [gather_turned(): result = lax.all_gather(both, axis, axis=0, tiled=True)]
    all_gather x1 -> x0, waiting for transfers between devices: 87.3 us -> none  [gather_turned(): result = lax.all_gather(both, axis, axis=0, tiled=True)]
    all_to_all x3, waiting for transfers between devices: 14.4 us -> 68.8 us  [sent_to_all(): return lax.all_to_all(copies, axis, split_axis=0, concat_axis=0, tiled=True)]
    all_to_all x3, blocking collectives: 100 us -> 60.7 us  [summed_on_arrival(): lax.all_to_all(blocks, axis, split_axis=0, concat_axis=0, tiled=True)]
    all_to_all x0 -> x2, starting transfers between devices: none -> 21.1 us  [gather_turned(): lax.all_to_all(jnp.stack([both] * lax.axis_size(axis)), axis, 0, 0)]
    all_to_all x3, starting transfers between devices: 26.6 us -> 21 us  [sent_to_all(): return lax.all_to_all(copies, axis, split_axis=0, concat_axis=0, tiled=True)]
  transfers between devices with their start and end apart: 5 -> 6, of which waited for: 3 -> 5; matrix products, arithmetic and copies ran while one was open for 5% -> 5% of each run, Pallas kernels for 0% -> 0%
where the time goes in v1:
time: 483 us; the launch traced here: 482 us
  waiting for transfers between devices  311 us (64%)
  blocking collectives  79.1 us (16%)
  starting transfers between devices  42.1 us (9%)
  matrix products  20.5 us (4%)
  between operations  14.5 us (3%)
  local copies, waits for them, and re-layouts  8.81 us (2%)
  other arithmetic  6.1 us (1%)
    all_to_all x2, waiting for transfers between devices, gather_turned(): lax.all_to_all(jnp.stack([both] * lax.axis_size(axis)), axis, 0, 0)  242 us
    all_to_all x3, waiting for transfers between devices, sent_to_all(): return lax.all_to_all(copies, axis, split_axis=0, concat_axis=0, tiled=True)  68.8 us
    all_to_all x3, blocking collectives, summed_on_arrival(): lax.all_to_all(blocks, axis, split_axis=0, concat_axis=0, tiled=True)  60.7 us
    all_to_all x2, starting transfers between devices, gather_turned(): lax.all_to_all(jnp.stack([both] * lax.axis_size(axis)), axis, 0, 0)  21.1 us
    all_to_all x3, starting transfers between devices, sent_to_all(): return lax.all_to_all(copies, axis, split_axis=0, concat_axis=0, tiled=True)  21 us
    all_to_all x1, blocking collectives, sent_to_all(): return lax.all_to_all(copies, axis, split_axis=0, concat_axis=0, tiled=True)  18.4 us
  transfers between devices with their start and end apart: 6, of which 5 were waited for; matrix products, arithmetic and copies ran while one was open for 5% of the time, Pallas kernels for 0%

profile of v1, /device:TPU:1, one launch (start us, length us, event | category | flops | bytes accessed | tf_op | source)
XLA Modules:
  0.0 482.1 jit_solution(14007644322571207614)
XLA Ops:
  6.5 0.7 pad_maximum_fusion.2
  7.3 0.7 reshape.455
  8.0 16.1 %all-to-all-start.2 = ((f32[32,1,128]{2,1,0:T(1,128)}), f32[32,1,128]{2,1,0:T(1,128)S(1)}, u32[]{:S(2)}, u32[]{:S(2)}) async-start(f32[32,1,128]{2,1,0:T(1,128)} %reshape.455), calls=%async_computation.2 | async-start | bytes 32768 | tf_op jit(solution)/shard_map/all_to_all | solution.py:18
  24.1 0.9 fusion.124
  25.0 1.0 fusion.108
  26.0 1.0 fusion.110
  27.0 8.4 %all-to-all-done.2 = f32[32,1,128]{2,1,0:T(1,128)S(1)} async-done(((f32[32,1,128]{2,1,0:T(1,128)}), f32[32,1,128]{2,1,0:T(1,128)S(1)}, u32[]{:S(2)}, u32[]{:S(2)}) %all-to-all-start.2) | async-done | bytes 16416 | tf_op jit(solution)/shard_map/all_to_all | solution.py:18
  35.5 1.1 broadcast_in_dim.17
  36.5 6.4 %all-to-all-start = ((bf16[8,32,2048]{2,1,0:T(8,128)(2,1)}), bf16[8,32,2048]{2,1,0:T(8,128)(2,1)S(1)}, u32[]{:S(2)}, u32[]{:S(2)}) async-start(bf16[8,32,2048]{2,1,0:T(8,128)(2,1)} %broadcast_in_dim.17), calls=%async_computation | async-start | bytes 2097152 | tf_op jit(solution)/shard_map/all_to_all | solution.py:31
  43.0 14.9 %all-to-all-done = bf16[8,32,2048]{2,1,0:T(8,128)(2,1)S(1)} async-done(((bf16[8,32,2048]{2,1,0:T(8,128)(2,1)}), bf16[8,32,2048]{2,1,0:T(8,128)(2,1)S(1)}, u32[]{:S(2)}, u32[]{:S(2)}) %all-to-all-start) | async-done | bytes 1048608 | tf_op jit(solution)/shard_map/all_to_all | solution.py:31
  57.9 2.8 stack.4
  60.7 5.0 %all-to-all-start.1 = ((bf16[32,64,1152]{2,1,0:T(8,128)(2,1)}), bf16[32,64,1152]{2,1,0:T(8,128)(2,1)}, u32[]{:S(2)}, u32[]{:S(2)}) async-start(bf16[32,64,1152]{2,1,0:T(8,128)(2,1)} %stack.4), calls=%async_computation.1 | async-start | bytes 9437184 | tf_op jit(solution)/shard_map/all_to_all | solution.py:18
  65.9 0.6 pad_maximum_fusion.1
  66.5 0.5 broadcast.260
  67.0 0.6 reduce.5
  67.8 233.5 %all-to-all-done.1 = bf16[32,64,1152]{2,1,0:T(8,128)(2,1)} async-done(((bf16[32,64,1152]{2,1,0:T(8,128)(2,1)}), bf16[32,64,1152]{2,1,0:T(8,128)(2,1)}, u32[]{:S(2)}, u32[]{:S(2)}) %all-to-all-start.1) | async-done | bytes 4718624 | tf_op jit(solution)/shard_map/all_to_all | solution.py:18
  301.3 2.1 fusion.63
  303.5 3.2 fusion.51
  306.7 21.9 %all_to_all.45 = bf16[8,32,2048]{2,1,0:T(8,128)(2,1)S(1)} all-to-all(bf16[8,32,2048]{2,1,0:T(8,128)(2,1)S(1)} %bitcast.138), channel_id=1, replica_groups=mesh['rep'=2,'fs'=32,'tp'=8] {'tp'}, dimensions={0} | all-to-all | bytes 2097152 | tf_op jit(solution)/shard_map/all_to_all | solution.py:53
  329.0 1.1 broadcast_in_dim.21
  330.2 4.5 all-to-all-start.4
  335.4 14.3 %all-to-all-done.4 = bf16[8,32,2048]{2,1,0:T(8,128)(2,1)S(1)} async-done(((bf16[8,32,2048]{2,1,0:T(8,128)(2,1)}), bf16[8,32,2048]{2,1,0:T(8,128)(2,1)S(1)}, u32[]{:S(2)}, u32[]{:S(2)}) %all-to-all-start.4) | async-done | bytes 1048608 | tf_op jit(solution)/shard_map/all_to_all | solution.py:31
  349.7 1.1 broadcast_in_dim.22
  350.8 10.1 %all-to-all-start.5 = ((bf16[32,256,64]{1,2,0:T(8,128)(2,1)}), bf16[32,256,64]{1,2,0:T(8,128)(2,1)S(1)}, u32[]{:S(2)}, u32[]{:S(2)}) async-start(bf16[32,256,64]{1,2,0:T(8,128)(2,1)} %broadcast_in_dim.22), calls=%async_computation.5 | async-start | bytes 2097152 | tf_op jit(solution)/shard_map/all_to_all | solution.py:31
  361.0 1.7 fusion.92
  362.7 1.7 fusion.93
  364.4 1.7 fusion.94
  366.1 4.5 while.15
  366.1 0.3 fusion.152
  366.4 0.3 fusion.153
  366.7 0.5 fusion.151
  367.2 0.3 fusion.152
  367.5 0.3 fusion.153
  367.8 0.5 fusion.151
  368.3 0.3 fusion.152
  368.6 0.3 fusion.153
  368.9 0.5 fusion.151
  369.4 0.3 fusion.152
  369.7 0.3 fusion.153
  370.0 0.5 fusion.151
  371.0 39.7 %all-to-all-done.5 = bf16[32,256,64]{1,2,0:T(8,128)(2,1)S(1)} async-done(((bf16[32,256,64]{1,2,0:T(8,128)(2,1)}), bf16[32,256,64]{1,2,0:T(8,128)(2,1)S(1)}, u32[]{:S(2)}, u32[]{:S(2)}) %all-to-all-start.5) | async-done | bytes 1048608 | tf_op jit(solution)/shard_map/all_to_all | solution.py:31
  410.7 0.5 fusion.50
  411.2 20.4 %all_to_all.46 = bf16[8,32,2048]{2,1,0:T(8,128)(2,1)S(1)} all-to-all(bf16[8,32,2048]{2,1,0:T(8,128)(2,1)S(1)} %bitcast.128), channel_id=1, replica_groups=mesh['rep'=2,'fs'=32,'tp'=8] {'tp'}, dimensions={0} | all-to-all | bytes 2097152 | tf_op jit(solution)/shard_map/all_to_all | solution.py:53
  432.2 18.4 %all_to_all.47 = bf16[8,32,2048]{2,1,0:T(8,128)(2,1)S(1)} all-to-all(bf16[8,32,2048]{2,1,0:T(8,128)(2,1)S(1)} %broadcast_in_dim.23), channel_id=1, replica_groups=mesh['rep'=2,'fs'=32,'tp'=8] {'tp'}, dimensions={0} | all-to-all | bytes 2097152 | tf_op jit(solution)/shard_map/all_to_all | solution.py:31
  450.6 2.1 fusion.66
  452.7 3.3 fusion.52
  456.0 18.4 %all_to_all.48 = bf16[8,32,2048]{2,1,0:T(8,128)(2,1)S(1)} all-to-all(bf16[8,32,2048]{2,1,0:T(8,128)(2,1)S(1)} %bitcast.137), channel_id=1, replica_groups=mesh['rep'=2,'fs'=32,'tp'=8] {'tp'}, dimensions={0} | all-to-all | bytes 2097152 | tf_op jit(solution)/shard_map/all_to_all | solution.py:53
  474.5 0.7 add_convert_fusion
  (67 shorter events, 2.0 us)
Async XLA Ops:
  6.5 36.4 %copy-start.1 = (f32[64,384]{1,0:T(8,128)S(1)}, f32[64,384]{1,0:T(8,128)}, u32[]{:S(2)}) copy-start(f32[64,384]{1,0:T(8,128)} %param.22) | copy-start | bytes 294916
  6.5 36.4 %copy-start.2 = (f32[64,384]{1,0:T(8,128)S(1)}, f32[64,384]{1,0:T(8,128)}, u32[]{:S(2)}) copy-start(f32[64,384]{1,0:T(8,128)} %param.24) | copy-start | bytes 294916
  6.5 36.5 %copy-start.3 = (f32[384,64]{0,1:T(8,128)S(1)}, f32[384,64]{0,1:T(8,128)}, u32[]{:S(2)}) copy-start(f32[384,64]{0,1:T(8,128)} %param.26) | copy-start | bytes 294916
  8.0 27.5 %all-to-all-start.2 = ((f32[32,1,128]{2,1,0:T(1,128)}), f32[32,1,128]{2,1,0:T(1,128)S(1)}, u32[]{:S(2)}, u32[]{:S(2)}) async-start(f32[32,1,128]{2,1,0:T(1,128)} %reshape.455), calls=%async_computation.2 | async-start | bytes 32768 | tf_op jit(solution)/shard_map/all_to_all | solution.py:18
  36.5 21.4 %all-to-all-start = ((bf16[8,32,2048]{2,1,0:T(8,128)(2,1)}), bf16[8,32,2048]{2,1,0:T(8,128)(2,1)S(1)}, u32[]{:S(2)}, u32[]{:S(2)}) async-start(bf16[8,32,2048]{2,1,0:T(8,128)(2,1)} %broadcast_in_dim.17), calls=%async_computation | async-start | bytes 2097152 | tf_op jit(solution)/shard_map/all_to_all | solution.py:31
  60.7 5.1 %copy-start.4 = (f32[64,256]{1,0:T(8,128)S(1)}, f32[64,256]{1,0:T(8,128)}, u32[]{:S(2)}) copy-start(f32[64,256]{1,0:T(8,128)} %param.28) | copy-start | bytes 196612
  60.7 5.1 %copy-start.5 = (f32[64,256]{1,0:T(8,128)S(1)}, f32[64,256]{1,0:T(8,128)}, u32[]{:S(2)}) copy-start(f32[64,256]{1,0:T(8,128)} %param.30) | copy-start | bytes 196612
  60.7 5.1 %copy-start.6 = (f32[64,256]{1,0:T(8,128)S(1)}, f32[64,256]{1,0:T(8,128)}, u32[]{:S(2)}) copy-start(f32[64,256]{1,0:T(8,128)} %param.32) | copy-start | bytes 196612
  60.7 240.6 %copy-start.9 = (f32[384]{0:T(512)S(1)}, f32[384]{0:T(512)}, u32[]{:S(2)}) copy-start(f32[384]{0:T(512)} %param.23) | copy-start | bytes 4612
  60.7 240.6 %all-to-all-start.1 = ((bf16[32,64,1152]{2,1,0:T(8,128)(2,1)}), bf16[32,64,1152]{2,1,0:T(8,128)(2,1)}, u32[]{:S(2)}, u32[]{:S(2)}) async-start(bf16[32,64,1152]{2,1,0:T(8,128)(2,1)} %stack.4), calls=%async_computation.1 | async-start | bytes 9437184 | tf_op jit(solution)/shard_map/all_to_all | solution.py:18
  65.7 295.2 %all-gather.2.cloned.1.call-start = ((), (), s32[]{:S(2)}) async-start(), calls=%async_computation.9 | async-start | bytes 3244032 | tf_op jit(solution)/shard_map/all_gather | solution.py:59
  65.9 237.6 %copy-start.10 = (f32[384]{0:T(512)S(1)}, f32[384]{0:T(512)}, u32[]{:S(2)}) copy-start(f32[384]{0:T(512)} %param.25) | copy-start | bytes 4612
  306.7 22.0 %copy-start = (bf16[32,2048]{1,0:T(8,128)(2,1)S(1)}, bf16[32,2048]{1,0:T(8,128)(2,1)}, u32[]{:S(2)}) copy-start(bf16[32,2048]{1,0:T(8,128)(2,1)} %param.20) | copy-start | bytes 393220
  328.8 6.6 %copy-start.7 = (f32[256,64]{0,1:T(8,128)S(1)}, f32[256,64]{0,1:T(8,128)}, u32[]{:S(2)}) copy-start(f32[256,64]{0,1:T(8,128)} %param.34) | copy-start | bytes 196612
  330.2 19.5 %all-to-all-start.4 = ((bf16[8,32,2048]{2,1,0:T(8,128)(2,1)}), bf16[8,32,2048]{2,1,0:T(8,128)(2,1)S(1)}, u32[]{:S(2)}, u32[]{:S(2)}) async-start(bf16[8,32,2048]{2,1,0:T(8,128)(2,1)} %broadcast_in_dim.21), calls=%async_computation.4 | async-start | bytes 2097152 | tf_op jit(solution)/shard_map/all_to_all | solution.py:31
  334.7 26.3 %copy-start.11 = (f32[256]{0:T(256)S(1)}, f32[256]{0:T(256)}, u32[]{:S(2)}) copy-start(f32[256]{0:T(256)} %param.31) | copy-start | bytes 3076
  350.8 11.8 %copy-start.12 = (f32[256]{0:T(256)S(1)}, f32[256]{0:T(256)}, u32[]{:S(2)}) copy-start(f32[256]{0:T(256)} %param.33) | copy-start | bytes 3076
  350.8 59.9 %all-to-all-start.5 = ((bf16[32,256,64]{1,2,0:T(8,128)(2,1)}), bf16[32,256,64]{1,2,0:T(8,128)(2,1)S(1)}, u32[]{:S(2)}, u32[]{:S(2)}) async-start(bf16[32,256,64]{1,2,0:T(8,128)(2,1)} %broadcast_in_dim.22), calls=%async_computation.5 | async-start | bytes 2097152 | tf_op jit(solution)/shard_map/all_to_all | solution.py:31
  361.0 3.4 copy-start.13
  366.0 44.7 %copy-start.8 = (f32[256]{0:T(256)S(1)}, f32[256]{0:T(256)}, u32[]{:S(2)}) copy-start(f32[256]{0:T(256)} %param.36) | copy-start | bytes 3076
Sparse Core Ops, SparseCore 0:
  68.6 215.4 all-gather.1
